TPU v7x, 32 devices: a whole 2x2x4 slice. The times are simulated.
32 devices in a mesh: ep: 4 (over y, x), tp: 8 (over z, core).
Axes of the slice: x: 2, y: 2, z: 4, core: 2. Of those that a mesh axis runs over, the one named last changes fastest.
Arguments:
- tokens: bfloat16 [1024, 2048], P('ep', 'tp'), may hold values from -600 to 600
- pre_gain: float32 [2048], P('tp'), may hold values from 0.1 to 1.9
- expert_gate: bfloat16 [4, 2048, 8192], P('ep', None, 'tp'), may hold values from -0.125 to 0.125
- expert_up: bfloat16 [4, 2048, 8192], P('ep', None, 'tp'), may hold values from -0.125 to 0.125
- expert_down: bfloat16 [4, 8192, 2048], P('ep', 'tp'), may hold values from -8 to 8
- routes: int32 [1024, 2], P('ep'), may hold values from 0 to 3, all different within a row; in each aligned block of 256 rows (0 to 255, 256 to 511, ...) at most 192 rows name the same one
- route_weights: float32 [1024, 2], P('ep'), may hold values from 0.1 to 1
- post_gain: float32 [2048], P('tp'), may hold values from 0.1 to 1.9
Outputs:
- layer_out: bfloat16 [1024, 2048], P('ep', 'tp')
Inputs may be any that keep to these rules, and one draw needn't show every extreme that they name: `routes`: each token names 2 different experts. Among the 256 tokens of one index of ep no expert is named more than 192 times, a bound that some expert reaches in some of these blocks.
All inputs are finite; a program needn't handle non-finite values.
Results may differ from a plain program's by a relative error of at most 0.024.
Values may be sent and summed in bfloat16 or wider, within the bound.
A program may use at most 64 MiB of HBM per device.

v0:
```python
import jax
import jax.numpy as jnp
from jax import lax
from jax.sharding import PartitionSpec as P

EPSILON = 1e-06


def local(tokens, pre_gain, expert_gate, expert_up, expert_down, routes, route_weights, post_gain):
    local_experts = expert_gate.shape[0]
    groups = lax.axis_size("ep")
    experts_all = local_experts * groups
    tok_rows, part_width = tokens.shape
    full_width = part_width * lax.axis_size("tp")
    capacity = 3 * tok_rows // experts_all
    values = tokens.astype(jnp.float32)
    input_sq = lax.psum(jnp.sum(values * values, axis=-1), "tp")
    normed = (
        values * lax.rsqrt(input_sq / full_width + EPSILON)[:, None] * pre_gain[None, :]
    ).astype(jnp.bfloat16)
    onehot = (routes[:, :, None] == jnp.arange(experts_all, dtype=jnp.int32)).astype(jnp.int32)
    onehot = onehot.reshape(tok_rows * 2, experts_all)
    earlier = jnp.cumsum(onehot, axis=0) - onehot
    slots = jnp.sum(earlier * onehot, axis=-1).reshape(tok_rows, 2)
    positions = routes * capacity + slots
    places = jnp.arange(experts_all * capacity, dtype=jnp.int32)
    first_pick = (places[:, None] == positions[None, :, 0]).astype(jnp.bfloat16)
    second_pick = (places[:, None] == positions[None, :, 1]).astype(jnp.bfloat16)
    dispatch = first_pick + second_pick
    outgoing = jnp.dot(dispatch, normed, preferred_element_type=jnp.float32).astype(jnp.bfloat16)
    arrived = lax.all_to_all(outgoing, "ep", split_axis=0, concat_axis=0, tiled=True)
    fragment = lax.all_gather(arrived, "tp", axis=1, tiled=True)
    count = fragment.shape[1]
    grouped = fragment.reshape(groups, local_experts, capacity, count)
    gate_pre = jnp.einsum(
        "secw,ewf->secf", grouped, expert_gate, preferred_element_type=jnp.float32
    )
    up_pre = jnp.einsum("secw,ewf->secf", grouped, expert_up, preferred_element_type=jnp.float32)
    hidden = (jax.nn.silu(gate_pre) * up_pre).astype(jnp.bfloat16)
    product = jnp.einsum("secf,efd->dsec", hidden, expert_down, preferred_element_type=jnp.float32)
    summed = lax.psum_scatter(
        product.reshape(lax.axis_size("tp") * part_width, groups * local_experts * capacity).astype(
            jnp.bfloat16
        ),
        "tp",
        scatter_dimension=0,
        tiled=True,
    )
    returned = lax.all_to_all(summed, "ep", split_axis=1, concat_axis=1, tiled=True)
    contract = (((0,), (1,)), ((), ()))
    first_out = lax.dot_general(first_pick, returned, contract, preferred_element_type=jnp.float32)
    second_out = lax.dot_general(
        second_pick, returned, contract, preferred_element_type=jnp.float32
    )
    combined = route_weights[:, 0:1] * first_out + route_weights[:, 1:2] * second_out
    output_sq = lax.psum(jnp.sum(combined * combined, axis=-1), "tp")
    scaled = combined * lax.rsqrt(output_sq / full_width + EPSILON)[:, None] * post_gain[None, :]
    return scaled.astype(jnp.bfloat16)


def solution(mesh):
    placed = (
        P("ep", "tp"),
        P("tp"),
        P("ep", None, "tp"),
        P("ep", None, "tp"),
        P("ep", "tp", None),
        P("ep", None),
        P("ep", None),
        P("tp"),
    )
    return jax.shard_map(
        local, mesh=mesh, in_specs=placed, out_specs=P("ep", "tp"), check_vma=False
    )
```

profile of v0, /device:TPU:0, one launch (start us, length us, event | category | flops | bytes accessed | tf_op | source)
XLA Modules:
  0.0 164.0 jit_solution(8557718616161930768)
XLA Ops:
  6.5 0.8 copy.20
  7.4 0.1 eq.61
  7.5 0.1 eq.57
  7.7 1.2 reduce-window.6
  8.9 0.2 slice_reduce_fusion
  9.1 0.2 reduce-window.9
  9.4 0.1 reshape.55
  9.6 0.7 multiply_add_fusion
  10.3 1.0 fusion.28
  11.3 18.1 %psum.14 = f32[256]{0:T(256)S(1)} all-reduce(f32[256]{0:T(256)S(1)} %fusion.28), channel_id=1, replica_groups=mesh['ep'=4,'tp'=8] {'tp'}, use_global_device_ids=true, to_apply=%region_4.5 | all-reduce | flops 256 | bytes 2048 | tf_op jit(solution)/shard_map/psum | solution.py:17
  29.4 1.3 convolution_convert_fusion
  30.7 10.1 %all_to_all.24 = bf16[4,192,256]{2,1,0:T(8,128)(2,1)} all-to-all(bf16[4,192,256]{2,1,0:T(8,128)(2,1)S(1)} %bitcast.82), channel_id=1, replica_groups=mesh['ep'=4,'tp'=8] {'ep'}, dimensions={0} | all-to-all | bytes 786432 | tf_op jit(solution)/shard_map/all_to_all | solution.py:31
  40.8 35.9 %all-gather.2.cloned.1.call-done = bf16[768,2048]{1,0:T(8,128)(2,1)} async-done(((bf16[768,256]{1,0:T(8,128)(2,1)}), bf16[768,2048]{1,0:T(8,128)(2,1)}) %all-gather.2.cloned.1.call-update) | async-done | bytes 3145744 | tf_op jit(solution)/shard_map/all_gather | solution.py:32
  76.8 6.3 %fusion.2 = f32[4,192,1024]{2,1,0:T(8,128)S(1)} fusion(bf16[4,192,2048]{2,1,0:T(8,128)(2,1)} %bitcast.90, bf16[1,2048,1024]{2,1,0:T(8,128)(2,1)} %param.11), kind=kOutput, calls=%fused_computation.2 | convolution fusion | flops 3221225472 | bytes 10485760 | tf_op jit(solution)/shard_map/secw,ewf->secf/dot_general | solution.py:38
  83.1 3.8 %fusion.9 = bf16[4,1,192,1024]{3,2,0,1:T(8,128)(2,1)S(1)} fusion(f32[4,192,1024]{2,1,0:T(8,128)S(1)} %fusion.2, bf16[4,192,2048]{2,1,0:T(8,128)(2,1)S(1)} %bitcast.91, bf16[1,2048,1024]{2,1,0:T(8,128)(2,1)S(1)} %copy-done.2), kind=kOutput, calls=%fused_computation.8 | convolution fusion | flops 3225944064 | bytes 12058624 | tf_op jit(solution)/shard_map/secw,ewf->secf/dot_general | solution.py:35
  87.0 4.8 %fusion.13 = bf16[2048,768]{0,1:T(8,128)(2,1)} fusion(bf16[768,1024]{1,0:T(8,128)(2,1)S(1)} %bitcast.92, bf16[1,1024,2048]{2,1,0:T(8,128)(2,1)S(1)} %copy-done.3), kind=kOutput, calls=%fused_computation.14 | convolution fusion | flops 3222798336 | bytes 8912896 | tf_op jit(solution)/shard_map/secf,efd->dsec/dot_general | solution.py:40
  91.8 38.8 %reduce-scatter.2.cloned.1.call-done = bf16[256,768]{0,1:T(8,128)(2,1)} async-done(((bf16[2048,768]{0,1:T(8,128)(2,1)}), bf16[256,768]{0,1:T(8,128)(2,1)}) %reduce-scatter.2.cloned.1.call-update) | async-done | bytes 393232 | tf_op jit(solution)/shard_map/reduce_scatter | solution.py:41
  130.6 3.6 %all-to-all-start.1 = ((bf16[256,4,192]{0,2,1:T(8,128)(2,1)}), bf16[256,4,192]{0,2,1:T(8,128)(2,1)S(1)}, u32[]{:S(2)}, u32[]{:S(2)}) async-start(bf16[256,4,192]{0,2,1:T(8,128)(2,1)} %bitcast.81), calls=%async_computation.2 | async-start | bytes 786432 | tf_op jit(solution)/shard_map/all_to_all | solution.py:49
  134.2 5.9 %all-to-all-done.1 = bf16[256,4,192]{0,2,1:T(8,128)(2,1)S(1)} async-done(((bf16[256,4,192]{0,2,1:T(8,128)(2,1)}), bf16[256,4,192]{0,2,1:T(8,128)(2,1)S(1)}, u32[]{:S(2)}, u32[]{:S(2)}) %all-to-all-start.1) | async-done | bytes 393248 | tf_op jit(solution)/shard_map/all_to_all | solution.py:49
  140.1 0.4 convolution_multiply_fusion.1
  140.5 0.4 multiply_reduce_fusion
  140.9 15.4 %psum.15 = f32[256]{0:T(256)S(1)} all-reduce(f32[256]{0:T(256)S(1)} %get-tuple-element.9), channel_id=1, replica_groups=mesh['ep'=4,'tp'=8] {'tp'}, use_global_device_ids=true, to_apply=%region_7.8 | all-reduce | flops 256 | bytes 2048 | tf_op jit(solution)/shard_map/psum | solution.py:56
  156.3 0.1 multiply_convert_fusion
  156.4 0.8 copy.23
  (22 shorter events, 0.3 us)
Async XLA Ops:
  6.5 70.3 %all-gather.2.cloned.1.call-start = ((), (), s32[]{:S(2)}) async-start(), calls=%async_computation.3 | async-start | bytes 3538944 | tf_op jit(solution)/shard_map/all_gather | solution.py:32
  40.8 89.8 %reduce-scatter.2.cloned.1.call-start = ((), (), s32[]{:S(2)}) async-start(), calls=%async_computation.4 | async-start | bytes 3538944 | tf_op jit(solution)/shard_map/reduce_scatter | solution.py:41
  76.8 6.3 %copy-start.2 = (bf16[1,2048,1024]{2,1,0:T(8,128)(2,1)S(1)}, bf16[1,2048,1024]{2,1,0:T(8,128)(2,1)}, u32[]{:S(2)}) copy-start(bf16[1,2048,1024]{2,1,0:T(8,128)(2,1)} %param.10) | copy-start | bytes 12582916
  76.8 6.3 %copy-start.4 = (bf16[768,2048]{1,0:T(8,128)(2,1)S(1)}, bf16[768,2048]{1,0:T(8,128)(2,1)}, u32[]{:S(2)}) copy-start(bf16[768,2048]{1,0:T(8,128)(2,1)} %all-gather.2.cloned.1.call-done) | copy-start | bytes 9437188
  83.1 3.9 %copy-start.3 = (bf16[1,1024,2048]{2,1,0:T(8,128)(2,1)S(1)}, bf16[1,1024,2048]{2,1,0:T(8,128)(2,1)}, u32[]{:S(2)}) copy-start(bf16[1,1024,2048]{2,1,0:T(8,128)(2,1)} %param.12) | copy-start | bytes 12582916
  91.8 42.4 %copy-start = (f32[256,2]{0,1:T(2,128)S(1)}, f32[256,2]{0,1:T(2,128)}, u32[]{:S(2)}) copy-start(f32[256,2]{0,1:T(2,128)} %param.14) | copy-start | bytes 6148
  91.8 64.5 %copy-start.1 = (f32[256]{0:T(256)S(1)}, f32[256]{0:T(256)}, u32[]{:S(2)}) copy-start(f32[256]{0:T(256)} %param.15) | copy-start | bytes 3076
  130.6 9.5 %all-to-all-start.1 = ((bf16[256,4,192]{0,2,1:T(8,128)(2,1)}), bf16[256,4,192]{0,2,1:T(8,128)(2,1)S(1)}, u32[]{:S(2)}, u32[]{:S(2)}) async-start(bf16[256,4,192]{0,2,1:T(8,128)(2,1)} %bitcast.81), calls=%async_computation.2 | async-start | bytes 786432 | tf_op jit(solution)/shard_map/all_to_all | solution.py:49
Sparse Core Ops, SparseCore 0:
  40.9 35.8 all-gather.1
  91.9 38.5 reduce-scatter.1
where the time goes:
time: 164 us
  waiting for transfers between devices  80.6 us (49%)
  blocking collectives  43.6 us (27%)
  matrix products  17 us (10%)
  between operations  13.5 us (8%)
  starting transfers between devices  3.69 us (2%)
  other arithmetic  3.35 us (2%)
  local copies, waits for them, and re-layouts  2.31 us (1%)
    reduce_scatter x1, waiting for transfers between devices, local(): lax.psum_scatter(product.reshape(lax.axis_size('tp') * part_width, groups...  38.8 us
    all_gather x1, waiting for transfers between devices, local(): fragment = lax.all_gather(arrived, 'tp', axis=1, tiled=True)  35.9 us
    psum x1, blocking collectives, local(): input_sq = lax.psum(jnp.sum(values * values, axis=-1), 'tp')  18.1 us
    psum x1, blocking collectives, local(): output_sq = lax.psum(jnp.sum(combined * combined, axis=-1), 'tp')  15.4 us
    all_to_all x1, blocking collectives, local(): lax.all_to_all(outgoing, 'ep', split_axis=0, concat_axis=0, tiled=True)  10.1 us
    dot_general x1, matrix products, local(): jnp.einsum('secw,ewf->secf', grouped, expert_up, preferred_element_type=j...  6.28 us
    all_to_all x1, waiting for transfers between devices, local(): lax.all_to_all(summed, 'ep', split_axis=1, concat_axis=1, tiled=True)  5.87 us
    dot_general x1, matrix products, local(): jnp.einsum('secf,efd->dsec', hidden, expert_down, preferred_element_type=...  4.83 us
  transfers between devices with their start and end apart: 3, of which 3 were waited for; matrix products, arithmetic and copies ran while one was open for 0% of the time, Pallas kernels for 0%

commit v1 on v0

--- a/solution.py
+++ b/solution.py
@@ -53,7 +53,7 @@
         second_pick, returned, contract, preferred_element_type=jnp.float32
     )
     combined = route_weights[:, 0:1] * first_out + route_weights[:, 1:2] * second_out
-    output_sq = lax.psum(jnp.sum(combined * combined, axis=-1), "tp")
+    output_sq = jnp.sum(lax.all_gather(jnp.sum(combined * combined, axis=-1), "tp"), axis=0)
     scaled = combined * lax.rsqrt(output_sq / full_width + EPSILON)[:, None] * post_gain[None, :]
     return scaled.astype(jnp.bfloat16)
 

time: 164 us -> 159 us (0.970)
  blocking collectives: 43.6 us -> 38.4 us
    psum x1 -> x0, blocking collectives: 15.4 us -> none  [local(): output_sq = lax.psum(jnp.sum(combined * combined, axis=-1), 'tp')]
    all_gather x0 -> x1, blocking collectives: none -> 10.3 us  [local(): lax.all_gather(jnp.sum(combined * combined, axis=-1), 'tp')]
where the time goes in v1:
time: 159 us
  waiting for transfers between devices  80.6 us (51%)
  blocking collectives  38.4 us (24%)
  matrix products  17 us (11%)
  between operations  13.5 us (8%)
  starting transfers between devices  3.69 us (2%)
  other arithmetic  3.38 us (2%)
  local copies, waits for them, and re-layouts  2.31 us (1%)
    reduce_scatter x1, waiting for transfers between devices, local(): lax.psum_scatter(product.reshape(lax.axis_size('tp') * part_width, groups...  38.8 us
    all_gather x1, waiting for transfers between devices, local(): fragment = lax.all_gather(arrived, 'tp', axis=1, tiled=True)  35.9 us
    psum x1, blocking collectives, local(): input_sq = lax.psum(jnp.sum(values * values, axis=-1), 'tp')  18.1 us
    all_gather x1, blocking collectives, local(): lax.all_gather(jnp.sum(combined * combined, axis=-1), 'tp')  10.3 us
    all_to_all x1, blocking collectives, local(): lax.all_to_all(outgoing, 'ep', split_axis=0, concat_axis=0, tiled=True)  10.1 us
    dot_general x1, matrix products, local(): jnp.einsum('secw,ewf->secf', grouped, expert_up, preferred_element_type=j...  6.28 us
    all_to_all x1, waiting for transfers between devices, local(): lax.all_to_all(summed, 'ep', split_axis=1, concat_axis=1, tiled=True)  5.87 us
    dot_general x1, matrix products, local(): jnp.einsum('secf,efd->dsec', hidden, expert_down, preferred_element_type=...  4.83 us
  transfers between devices with their start and end apart: 3, of which 3 were waited for; matrix products, arithmetic and copies ran while one was open for 0% of the time, Pallas kernels for 0%

profile of v1, /device:TPU:0, one launch (start us, length us, event | category | flops | bytes accessed | tf_op | source)
XLA Modules:
  0.0 158.9 jit_solution(1153129783960446045)
XLA Ops:
  6.5 0.8 copy.25
  7.4 0.1 eq.61
  7.5 0.1 eq.57
  7.7 1.2 reduce-window.6
  8.9 0.2 slice_reduce_fusion
  9.1 0.2 reduce-window.9
  9.4 0.1 reshape.59
  9.6 0.7 multiply_add_fusion
  10.3 1.0 fusion.28
  11.3 18.1 %psum.7 = f32[256]{0:T(256)S(1)} all-reduce(f32[256]{0:T(256)S(1)} %fusion.28), channel_id=1, replica_groups=mesh['ep'=4,'tp'=8] {'tp'}, use_global_device_ids=true, to_apply=%region_4.5 | all-reduce | flops 256 | bytes 2048 | tf_op jit(solution)/shard_map/psum | solution.py:17
  29.4 1.3 convolution_convert_fusion
  30.7 10.1 %all_to_all.24 = bf16[4,192,256]{2,1,0:T(8,128)(2,1)} all-to-all(bf16[4,192,256]{2,1,0:T(8,128)(2,1)S(1)} %bitcast.83), channel_id=1, replica_groups=mesh['ep'=4,'tp'=8] {'ep'}, dimensions={0} | all-to-all | bytes 786432 | tf_op jit(solution)/shard_map/all_to_all | solution.py:31
  40.8 35.9 %all-gather.4.cloned.1.call-done = bf16[768,2048]{1,0:T(8,128)(2,1)} async-done(((bf16[768,256]{1,0:T(8,128)(2,1)}), bf16[768,2048]{1,0:T(8,128)(2,1)}) %all-gather.4.cloned.1.call-update) | async-done | bytes 3145744 | tf_op jit(solution)/shard_map/all_gather | solution.py:32
  76.8 6.3 %fusion.2 = f32[4,192,1024]{2,1,0:T(8,128)S(1)} fusion(bf16[4,192,2048]{2,1,0:T(8,128)(2,1)} %bitcast.92, bf16[1,2048,1024]{2,1,0:T(8,128)(2,1)} %param.11), kind=kOutput, calls=%fused_computation.2 | convolution fusion | flops 3221225472 | bytes 10485760 | tf_op jit(solution)/shard_map/secw,ewf->secf/dot_general | solution.py:38
  83.1 3.8 %fusion.9 = bf16[4,1,192,1024]{3,2,0,1:T(8,128)(2,1)S(1)} fusion(f32[4,192,1024]{2,1,0:T(8,128)S(1)} %fusion.2, bf16[4,192,2048]{2,1,0:T(8,128)(2,1)S(1)} %bitcast.93, bf16[1,2048,1024]{2,1,0:T(8,128)(2,1)S(1)} %copy-done.2), kind=kOutput, calls=%fused_computation.8 | convolution fusion | flops 3225944064 | bytes 12058624 | tf_op jit(solution)/shard_map/secw,ewf->secf/dot_general | solution.py:35
  87.0 4.8 %fusion.13 = bf16[2048,768]{0,1:T(8,128)(2,1)} fusion(bf16[768,1024]{1,0:T(8,128)(2,1)S(1)} %bitcast.94, bf16[1,1024,2048]{2,1,0:T(8,128)(2,1)S(1)} %copy-done.3), kind=kOutput, calls=%fused_computation.14 | convolution fusion | flops 3222798336 | bytes 8912896 | tf_op jit(solution)/shard_map/secf,efd->dsec/dot_general | solution.py:40
  91.8 38.8 %reduce-scatter.2.cloned.1.call-done = bf16[256,768]{0,1:T(8,128)(2,1)} async-done(((bf16[2048,768]{0,1:T(8,128)(2,1)}), bf16[256,768]{0,1:T(8,128)(2,1)}) %reduce-scatter.2.cloned.1.call-update) | async-done | bytes 393232 | tf_op jit(solution)/shard_map/reduce_scatter | solution.py:41
  130.6 3.6 %all-to-all-start.1 = ((bf16[256,4,192]{0,2,1:T(8,128)(2,1)}), bf16[256,4,192]{0,2,1:T(8,128)(2,1)S(1)}, u32[]{:S(2)}, u32[]{:S(2)}) async-start(bf16[256,4,192]{0,2,1:T(8,128)(2,1)} %bitcast.82), calls=%async_computation.2 | async-start | bytes 786432 | tf_op jit(solution)/shard_map/all_to_all | solution.py:49
  134.2 5.9 %all-to-all-done.1 = bf16[256,4,192]{0,2,1:T(8,128)(2,1)S(1)} async-done(((bf16[256,4,192]{0,2,1:T(8,128)(2,1)}), bf16[256,4,192]{0,2,1:T(8,128)(2,1)S(1)}, u32[]{:S(2)}, u32[]{:S(2)}) %all-to-all-start.1) | async-done | bytes 393248 | tf_op jit(solution)/shard_map/all_to_all | solution.py:49
  140.1 0.4 convolution_multiply_fusion.1
  140.5 0.4 multiply_reduce_fusion
  140.9 10.3 %all-gather.1 = f32[8,1,256]{2,1,0:T(1,128)S(1)} all-gather(f32[1,1,256]{2,1,0:T(1,128)S(1)} %bitcast.85), channel_id=2, replica_groups=mesh['ep'=4,'tp'=8] {'tp'}, dimensions={0}, use_global_device_ids=true | all-gather | bytes 9216 | tf_op jit(solution)/shard_map/all_gather | solution.py:56
  151.2 0.1 multiply_convert_fusion
  151.3 0.8 copy.28
  (23 shorter events, 0.3 us)
Async XLA Ops:
  6.5 70.3 %all-gather.4.cloned.1.call-start = ((), (), s32[]{:S(2)}) async-start(), calls=%async_computation.3 | async-start | bytes 3538944 | tf_op jit(solution)/shard_map/all_gather | solution.py:32
  40.8 89.8 %reduce-scatter.2.cloned.1.call-start = ((), (), s32[]{:S(2)}) async-start(), calls=%async_computation.4 | async-start | bytes 3538944 | tf_op jit(solution)/shard_map/reduce_scatter | solution.py:41
  76.8 6.3 %copy-start.2 = (bf16[1,2048,1024]{2,1,0:T(8,128)(2,1)S(1)}, bf16[1,2048,1024]{2,1,0:T(8,128)(2,1)}, u32[]{:S(2)}) copy-start(bf16[1,2048,1024]{2,1,0:T(8,128)(2,1)} %param.10) | copy-start | bytes 12582916
  76.8 6.3 %copy-start.4 = (bf16[768,2048]{1,0:T(8,128)(2,1)S(1)}, bf16[768,2048]{1,0:T(8,128)(2,1)}, u32[]{:S(2)}) copy-start(bf16[768,2048]{1,0:T(8,128)(2,1)} %all-gather.4.cloned.1.call-done) | copy-start | bytes 9437188
  83.1 3.9 %copy-start.3 = (bf16[1,1024,2048]{2,1,0:T(8,128)(2,1)S(1)}, bf16[1,1024,2048]{2,1,0:T(8,128)(2,1)}, u32[]{:S(2)}) copy-start(bf16[1,1024,2048]{2,1,0:T(8,128)(2,1)} %param.12) | copy-start | bytes 12582916
  91.8 42.4 %copy-start = (f32[256,2]{0,1:T(2,128)S(1)}, f32[256,2]{0,1:T(2,128)}, u32[]{:S(2)}) copy-start(f32[256,2]{0,1:T(2,128)} %param.14) | copy-start | bytes 6148
  91.8 59.4 %copy-start.1 = (f32[256]{0:T(256)S(1)}, f32[256]{0:T(256)}, u32[]{:S(2)}) copy-start(f32[256]{0:T(256)} %param.15) | copy-start | bytes 3076
  130.6 9.5 %all-to-all-start.1 = ((bf16[256,4,192]{0,2,1:T(8,128)(2,1)}), bf16[256,4,192]{0,2,1:T(8,128)(2,1)S(1)}, u32[]{:S(2)}, u32[]{:S(2)}) async-start(bf16[256,4,192]{0,2,1:T(8,128)(2,1)} %bitcast.82), calls=%async_computation.2 | async-start | bytes 786432 | tf_op jit(solution)/shard_map/all_to_all | solution.py:49
Sparse Core Ops, SparseCore 0:
  40.9 35.8 all-gather.3
  91.9 38.5 reduce-scatter.1
